TPU v7x, 32 devices: a whole 2x2x4 slice. The times are simulated.
32 devices in a mesh: grp: 2 (over y), sp: 4 (over z), tp: 4 (over x, core).
Axes of the slice: x: 2, y: 2, z: 4, core: 2. Of those that a mesh axis runs over, the one named last changes fastest.
Arguments:
- tokens: bfloat16 [2048, 4096], P(('grp', 'sp')), parts along dimension 0, may hold values from -6 to 6
- norm_gain: bfloat16 [2, 4096], replicated, may hold values from 0.099609375 to 1.8984375
- w_query: bfloat16 [2, 4096, 2048], P(None, 'sp', 'tp'), may hold values from -0.09375 to 0.09375
- w_key: bfloat16 [2, 4096, 2048], P(None, 'sp', 'tp'), may hold values from -0.09375 to 0.09375
- w_value: bfloat16 [2, 4096, 2048], P(None, 'sp', 'tp'), may hold values from -0.09375 to 0.09375
- w_out: bfloat16 [2, 2048, 4096], P(None, 'tp', 'sp'), may hold values from -0.125 to 0.125
- offset_bias: float32 [2, 16, 15, 31], P(None, 'tp'), may hold values from -4 to 300
Outputs:
- mixed: bfloat16 [2048, 4096], P(('grp', 'sp')), parts along dimension 0
There are 2 independent parts, one for each index of `grp`. A program takes and returns all parts, laid end to end along the dimension named above; an argument that names none is the same for every part. Nothing has to cross between parts.
All inputs are finite; a program needn't handle non-finite values.
Results may differ from a plain program's by a relative error of at most 0.013.
Values may be sent and summed in bfloat16 or wider, within the bound.
A program may use at most 128 MiB of HBM per device.

v0:
```python
import jax
import jax.numpy as jnp
from jax import lax
from jax.sharding import PartitionSpec as P

HD = 128
GRID_W = 64
KR = 8
KC = 16
LAYERS = 2


norm_eps = 1e-06


def with_halo(block, sides, width):
    for axis, dim in sides:
        count = lax.axis_size(axis)
        forward = [(i, i + 1) for i in range(count - 1)]
        backward = [(target, source) for source, target in forward]
        low = lax.ppermute(
            lax.slice_in_dim(block, block.shape[dim] - width, None, axis=dim), axis, forward
        )
        high = lax.ppermute(lax.slice_in_dim(block, 0, width, axis=dim), axis, backward)
        block = jnp.concatenate([low, block, high], axis=dim)
    return block


def rms_rows(values, gain):
    wide = values.astype(jnp.float32)
    scaled = wide * lax.rsqrt(jnp.mean(wide * wide, axis=-1, keepdims=True) + norm_eps)
    return (scaled * gain.astype(jnp.float32)).astype(jnp.bfloat16)


def on_device(tokens, norm_gain, w_query, w_key, w_value, w_out, offset_bias):
    sp_count = lax.axis_size("sp")
    sp_index = lax.axis_index("sp")
    tok_rows = tokens.shape[0]
    local_rows = tok_rows // GRID_W
    grid_rows = local_rows * sp_count
    heads_here = offset_bias.shape[1]
    head_width = heads_here * HD
    reach = KR // 2
    scale = HD ** (-0.5)
    columns = jnp.arange(GRID_W, dtype=jnp.int32)
    col_first = jnp.clip(columns - KC // 2, 0, GRID_W - KC)
    col_inside = (columns[None, :] >= col_first[:, None]) & (
        columns[None, :] < col_first[:, None] + KC
    )
    col_offset = jnp.clip(columns[None, :] - columns[:, None], 1 - KC, KC - 1) + KC - 1
    col_onehot = (
        jnp.arange(2 * KC - 1, dtype=jnp.int32)[:, None, None] == col_offset[None, :, :]
    ).astype(jnp.float32)
    first_row = sp_index * local_rows
    own_rows = first_row + jnp.arange(local_rows, dtype=jnp.int32)
    row_first = jnp.clip(own_rows - reach, 0, grid_rows - KR)
    band_start = row_first - first_row + reach
    row_offset = (
        row_first[:, None] + jnp.arange(KR, dtype=jnp.int32)[None, :] - own_rows[:, None] + KR - 1
    )
    row_onehot = (
        row_offset[:, :, None] == jnp.arange(2 * KR - 1, dtype=jnp.int32)[None, None, :]
    ).astype(jnp.float32)
    every_query, every_key, every_value, every_out = (
        lax.all_gather(w_query, "sp", axis=1, tiled=True),
        lax.all_gather(w_key, "sp", axis=1, tiled=True),
        lax.all_gather(w_value, "sp", axis=1, tiled=True),
        lax.all_gather(w_out, "sp", axis=2, tiled=True),
    )
    residual = tokens
    for layer_index in range(LAYERS):
        normed = rms_rows(residual, norm_gain[layer_index])
        queries = jnp.dot(normed, every_query[layer_index], preferred_element_type=jnp.float32)
        keys = jnp.dot(normed, every_key[layer_index], preferred_element_type=jnp.float32)
        values = jnp.dot(normed, every_value[layer_index], preferred_element_type=jnp.float32)
        out_weight = every_out[layer_index]
        queries = queries.astype(jnp.bfloat16).reshape(local_rows, GRID_W, heads_here, HD)
        key_values = jnp.concatenate(
            [keys.astype(jnp.bfloat16), values.astype(jnp.bfloat16)], axis=1
        )
        key_values = key_values.reshape(local_rows, GRID_W, 2 * head_width)
        padded = with_halo(key_values, (("sp", 0),), reach)
        bands = jax.vmap(lambda band_begin: lax.dynamic_slice_in_dim(padded, band_begin, KR, 0))(
            band_start
        )
        band_keys = bands[..., :head_width].reshape(local_rows, KR, GRID_W, heads_here, HD)
        band_values = bands[..., head_width:].reshape(local_rows, KR, GRID_W, heads_here, HD)
        col_bias = jnp.einsum(
            "hro,oqk->hrqk", offset_bias[layer_index], col_onehot, precision=lax.Precision.HIGHEST
        )
        full_bias = jnp.einsum(
            "ijr,hrqk->hiqjk", row_onehot, col_bias, precision=lax.Precision.HIGHEST
        )
        scores = jnp.einsum(
            "iqhd,ijkhd->hiqjk", queries, band_keys, preferred_element_type=jnp.float32
        )
        scores = scores * scale + full_bias
        scores = jnp.where(col_inside[None, None, :, None, :], scores, -jnp.inf)
        flattened = scores.reshape(heads_here, local_rows, GRID_W, KR * GRID_W)
        weights = jax.nn.softmax(flattened, axis=-1).astype(jnp.bfloat16)
        weights = weights.reshape(heads_here, local_rows, GRID_W, KR, GRID_W)
        attended = jnp.einsum(
            "hiqjk,ijkhd->iqhd", weights, band_values, preferred_element_type=jnp.float32
        )
        attended = attended.astype(jnp.bfloat16).reshape(tok_rows, head_width)
        branch = lax.psum(
            jnp.dot(attended, out_weight, preferred_element_type=jnp.float32).astype(jnp.bfloat16),
            "tp",
        ).astype(jnp.float32)
        residual = (residual.astype(jnp.float32) + branch).astype(jnp.bfloat16)
    return residual


def solution(mesh):
    return jax.shard_map(
        on_device,
        mesh=mesh,
        in_specs=(
            P(("grp", "sp"), None),
            P(),
            P(None, "sp", "tp"),
            P(None, "sp", "tp"),
            P(None, "sp", "tp"),
            P(None, "tp", "sp"),
            P(None, "tp", None, None),
        ),
        out_specs=P(("grp", "sp"), None),
        check_vma=False,
    )
```

profile of v0, /device:TPU:0, one launch (start us, length us, event | category | flops | bytes accessed | tf_op | source)
XLA Modules:
  0.0 783.5 jit_solution(1764364375646308337)
XLA Ops:
  6.5 0.7 all-gather.5.cloned.1.call-update
  7.3 0.0 all-gather.7.cloned.1.call-start
  7.3 0.7 all-gather.7.cloned.1.call-update
  8.0 0.0 all-gather.9.cloned.1.call-start
  8.1 0.7 all-gather.9.cloned.1.call-update
  8.7 0.0 all-gather.11.cloned.1.call-start
  8.8 0.5 all-gather.11.cloned.1.call-update
  9.3 0.0 all-reduce.4.cloned.1.call-start
  9.4 0.1 subtract_add_fusion
  9.5 0.1 fusion.70
  9.6 1.0 fusion.73
  10.7 3.8 fusion.30
  14.5 6.0 copy.16
  20.5 0.5 fusion
  21.1 140.2 %all-gather.5.cloned.1.call-done = bf16[2,4096,512]{2,1,0:T(8,128)(2,1)} async-done(((bf16[2,1024,512]{2,1,0:T(8,128)(2,1)}), bf16[2,4096,512]{2,1,0:T(8,128)(2,1)}) %all-gather.5.cloned.1.call-update) | async-done | bytes 8388624 | tf_op jit(solution)/shard_map/all_gather | solution.py:66
  161.3 3.5 fusion.54
  164.7 145.9 %all-gather.7.cloned.1.call-done = bf16[2,4096,512]{2,1,0:T(8,128)(2,1)} async-done(((bf16[2,1024,512]{2,1,0:T(8,128)(2,1)}), bf16[2,4096,512]{2,1,0:T(8,128)(2,1)}) %all-gather.7.cloned.1.call-update) | async-done | bytes 8388624 | tf_op jit(solution)/shard_map/all_gather | solution.py:67
  310.7 3.5 fusion.55
  314.2 0.1 pad_maximum_fusion.2
  314.2 2.1 collective-permute-start
  316.3 1.5 collective-permute-start.1
  317.8 149.6 %all-gather.9.cloned.1.call-done = bf16[2,4096,512]{2,1,0:T(8,128)(2,1)} async-done(((bf16[2,1024,512]{2,1,0:T(8,128)(2,1)}), bf16[2,4096,512]{2,1,0:T(8,128)(2,1)}) %all-gather.9.cloned.1.call-update) | async-done | bytes 8388624 | tf_op jit(solution)/shard_map/all_gather | solution.py:65
  467.4 3.5 fusion.56
  470.9 0.1 reshape.184
  471.0 2.5 pad_maximum_fusion
  473.5 4.4 gather_fusion
  477.9 3.5 slice_bitcast_fusion.19
  481.4 0.6 copy-done.2
  482.0 1.0 fusion.93
  483.0 0.7 fusion.16
  483.7 1.0 fusion.60
  484.7 0.2 copy.19
  484.9 132.0 %all-gather.11.cloned.1.call-done = bf16[2,512,4096]{2,1,0:T(8,128)(2,1)} async-done(((bf16[2,512,1024]{2,1,0:T(8,128)(2,1)}), bf16[2,512,4096]{2,1,0:T(8,128)(2,1)}) %all-gather.11.cloned.1.call-update) | async-done | bytes 8388624 | tf_op jit(solution)/shard_map/all_gather | solution.py:68
  616.9 4.8 convolution_convert_fusion.1
  621.7 0.0 all-reduce.4.cloned.1.call-update
  621.7 0.0 all-reduce.6.cloned.1.call-start
  621.8 2.4 fusion.71
  624.2 47.2 %all-reduce.4.cloned.1.call-done = bf16[256,4096]{1,0:T(8,128)(2,1)} async-done(((bf16[256,4096]{1,0:T(8,128)(2,1)}), bf16[256,4096]{1,0:T(8,128)(2,1)}) %all-reduce.4.cloned.1.call-update) | async-done | bytes 2097168 | tf_op jit(solution)/shard_map/psum | solution.py:106
  671.5 2.5 fusion.4
  674.0 1.0 fusion.6
  675.0 4.5 fusion.57
  679.5 0.1 slice-done.3
  679.5 1.2 fusion.58
  680.8 0.1 pad_maximum_fusion.3
  680.8 3.4 collective-permute-start.2
  684.3 1.5 collective-permute-start.3
  685.8 3.9 fusion.28
  689.7 5.8 copy.22
  695.4 4.8 fusion.59
  700.2 1.0 reshape.189
  701.3 2.4 pad_maximum_fusion.1
  703.6 4.2 gather_fusion.1
  707.8 3.1 slice_bitcast_fusion.17
  710.9 0.3 copy-done.3
  711.3 1.0 fusion.94
  712.3 0.7 fusion.17
  713.0 1.0 fusion.65
  714.0 0.2 copy.25
  714.2 0.2 slice-done
  714.5 1.5 slice-done.1
  715.9 2.6 convolution_convert_fusion
  718.5 0.0 all-reduce.6.cloned.1.call-update
  718.6 53.4 %all-reduce.6.cloned.1.call-done = bf16[256,4096]{1,0:T(8,128)(2,1)} async-done(((bf16[256,4096]{1,0:T(8,128)(2,1)}), bf16[256,4096]{1,0:T(8,128)(2,1)}) %all-reduce.6.cloned.1.call-update) | async-done | bytes 2097168 | tf_op jit(solution)/shard_map/psum | solution.py:106
  771.9 4.7 fusion.7
  (35 shorter events, 0.2 us)
Async XLA Ops:
  6.5 2.9 copy-start.7
  6.5 154.7 %all-gather.5.cloned.1.call-start = ((), (), s32[]{:S(2)}) async-start(), calls=%async_computation | async-start | bytes 10485760 | tf_op jit(solution)/shard_map/all_gather | solution.py:66
  7.3 303.4 %all-gather.7.cloned.1.call-start = ((), (), s32[]{:S(2)}) async-start(), calls=%async_computation.1 | async-start | bytes 10485760 | tf_op jit(solution)/shard_map/all_gather | solution.py:67
  8.0 459.4 %all-gather.9.cloned.1.call-start = ((), (), s32[]{:S(2)}) async-start(), calls=%async_computation.2 | async-start | bytes 10485760 | tf_op jit(solution)/shard_map/all_gather | solution.py:65
  8.7 608.2 %all-gather.11.cloned.1.call-start = ((), (), s32[]{:S(2)}) async-start(), calls=%async_computation.3 | async-start | bytes 10485760 | tf_op jit(solution)/shard_map/all_gather | solution.py:68
  9.3 662.1 %all-reduce.4.cloned.1.call-start = ((), (), s32[]{:S(2)}) async-start(), calls=%async_computation.4 | async-start | bytes 4194304 | tf_op jit(solution)/shard_map/psum | solution.py:106
  14.5 6.0 copy-start
  14.5 6.6 copy-start.6
  314.2 156.7 %collective-permute-start = (bf16[4,64,1024]{2,1,0:T(8,128)(2,1)S(1)}, bf16[4,64,1024]{2,1,0:T(8,128)(2,1)}, u32[]{:S(2)}, u32[]{:S(2)}) collective-permute-start(bf16[4,64,1024]{2,1,0:T(8,128)(2,1)S(1)} %bitcast.150), channel_id=1, source_target_pairs={{0,4},{4,8},{8,12},{1,5},{5,9},{9,13},{2,6},{6,10},{10,14},{3,7},{... | collective-permute-start | bytes 1572872 | tf_op jit(solution)/shard_map/ppermute | solution.py:21
  316.3 154.6 %collective-permute-start.1 = (bf16[4,64,1024]{2,1,0:T(8,128)(2,1)S(1)}, bf16[4,64,1024]{2,1,0:T(8,128)(2,1)}, u32[]{:S(2)}, u32[]{:S(2)}) collective-permute-start(bf16[4,64,1024]{2,1,0:T(8,128)(2,1)S(1)} %bitcast.151), channel_id=1, source_target_pairs={{4,0},{8,4},{12,8},{5,1},{9,5},{13,9},{6,2},{10,6},{14,10},{7,3},{... | collective-permute-start | bytes 1572872 | tf_op jit(solution)/shard_map/ppermute | solution.py:24
  477.9 4.1 copy-start.2
  621.7 150.2 %all-reduce.6.cloned.1.call-start = ((), (), s32[]{:S(2)}) async-start(), calls=%async_computation.5 | async-start | bytes 4194304 | tf_op jit(solution)/shard_map/psum | solution.py:106
  671.5 2.5 copy-start.1
  674.0 5.5 slice-start.2
  674.9 4.5 copy-start.5
  675.0 4.6 slice-start.3
  679.5 6.3 copy-start.4
  680.8 20.4 %collective-permute-start.2 = (bf16[4,64,1024]{2,1,0:T(8,128)(2,1)S(1)}, bf16[4,64,1024]{2,1,0:T(8,128)(2,1)S(1)}, u32[]{:S(2)}, u32[]{:S(2)}) collective-permute-start(bf16[4,64,1024]{2,1,0:T(8,128)(2,1)S(1)} %bitcast.147), channel_id=1, source_target_pairs={{0,4},{4,8},{8,12},{1,5},{5,9},{9,13},{2,6},{6,10},{10,14},{3,7},{... | collective-permute-start | bytes 1572872 | tf_op jit(solution)/shard_map/ppermute | solution.py:21
  684.3 17.0 %collective-permute-start.3 = (bf16[4,64,1024]{2,1,0:T(8,128)(2,1)S(1)}, bf16[4,64,1024]{2,1,0:T(8,128)(2,1)}, u32[]{:S(2)}, u32[]{:S(2)}) collective-permute-start(bf16[4,64,1024]{2,1,0:T(8,128)(2,1)S(1)} %bitcast.148), channel_id=1, source_target_pairs={{4,0},{8,4},{12,8},{5,1},{9,5},{13,9},{6,2},{10,6},{14,10},{7,3},{... | collective-permute-start | bytes 1572872 | tf_op jit(solution)/shard_map/ppermute | solution.py:24
  707.8 3.4 copy-start.3
  712.3 2.2 slice-start
  713.0 2.9 slice-start.1
Sparse Core Ops, SparseCore 0:
  8.9 152.3 all-gather.4
  162.8 147.7 all-gather.6
  312.2 155.1 all-gather.8
  468.8 148.0 all-gather.10
  621.9 49.5 all-reduce.3
  718.7 53.1 all-reduce.5
where the time goes:
time: 784 us; the launch traced here: 783 us
  waiting for transfers between devices  671 us (86%)
  matrix products  43.4 us (6%)
  local copies, waits for them, and re-layouts  31.2 us (4%)
  other arithmetic  15.4 us (2%)
  between operations  13.8 us (2%)
  starting transfers between devices  8.71 us (1%)
    all_gather x1, waiting for transfers between devices, on_device(): lax.all_gather(w_query, 'sp', axis=1, tiled=True)  150 us
    all_gather x1, waiting for transfers between devices, on_device(): lax.all_gather(w_value, 'sp', axis=1, tiled=True)  146 us
    all_gather x1, waiting for transfers between devices, on_device(): lax.all_gather(w_key, 'sp', axis=1, tiled=True)  140 us
    all_gather x1, waiting for transfers between devices, on_device(): lax.all_gather(w_out, 'sp', axis=2, tiled=True)  132 us
    psum x2, waiting for transfers between devices, on_device(): lax.psum(jnp.dot(attended, out_weight, preferred_element_type=jnp.float32...  101 us
  transfers between devices with their start and end apart: 10, of which 6 were waited for; matrix products, arithmetic and copies ran while one was open for 7% of the time, Pallas kernels for 0%

commit v1 on v0

--- a/solution.py
+++ b/solution.py
@@ -61,24 +61,25 @@
     row_onehot = (
         row_offset[:, :, None] == jnp.arange(2 * KR - 1, dtype=jnp.int32)[None, None, :]
     ).astype(jnp.float32)
-    every_query, every_key, every_value, every_out = (
-        lax.all_gather(w_query, "sp", axis=1, tiled=True),
-        lax.all_gather(w_key, "sp", axis=1, tiled=True),
-        lax.all_gather(w_value, "sp", axis=1, tiled=True),
-        lax.all_gather(w_out, "sp", axis=2, tiled=True),
-    )
-    residual = tokens
+    qkv_weight = jnp.concatenate([w_query, w_key, w_value], axis=2)
+    residual = lax.all_to_all(tokens, "sp", split_axis=1, concat_axis=0, tiled=True)
+    width = residual.shape[1]
+    features = width * sp_count
     for layer_index in range(LAYERS):
-        normed = rms_rows(residual, norm_gain[layer_index])
-        queries = jnp.dot(normed, every_query[layer_index], preferred_element_type=jnp.float32)
-        keys = jnp.dot(normed, every_key[layer_index], preferred_element_type=jnp.float32)
-        values = jnp.dot(normed, every_value[layer_index], preferred_element_type=jnp.float32)
-        out_weight = every_out[layer_index]
-        queries = queries.astype(jnp.bfloat16).reshape(local_rows, GRID_W, heads_here, HD)
-        key_values = jnp.concatenate(
-            [keys.astype(jnp.bfloat16), values.astype(jnp.bfloat16)], axis=1
+        wide = residual.astype(jnp.float32)
+        squares = lax.psum_scatter(
+            jnp.sum(wide * wide, axis=-1, keepdims=True), "sp", scatter_dimension=0, tiled=True
         )
-        key_values = key_values.reshape(local_rows, GRID_W, 2 * head_width)
+        inverse = lax.rsqrt(squares / features + norm_eps)
+        gain = lax.dynamic_slice_in_dim(norm_gain[layer_index], sp_index * width, width, 0)
+        gained = (wide * gain.astype(jnp.float32)).astype(jnp.bfloat16)
+        partial = jnp.dot(gained, qkv_weight[layer_index], preferred_element_type=jnp.float32)
+        mine = lax.psum_scatter(
+            partial.astype(jnp.bfloat16), "sp", scatter_dimension=0, tiled=True
+        )
+        mine = (mine.astype(jnp.float32) * inverse).astype(jnp.bfloat16)
+        queries = mine[:, :head_width].reshape(local_rows, GRID_W, heads_here, HD)
+        key_values = mine[:, head_width:].reshape(local_rows, GRID_W, 2 * head_width)
         padded = with_halo(key_values, (("sp", 0),), reach)
         bands = jax.vmap(lambda band_begin: lax.dynamic_slice_in_dim(padded, band_begin, KR, 0))(
             band_start
@@ -103,12 +104,11 @@
             "hiqjk,ijkhd->iqhd", weights, band_values, preferred_element_type=jnp.float32
         )
         attended = attended.astype(jnp.bfloat16).reshape(tok_rows, head_width)
-        branch = lax.psum(
-            jnp.dot(attended, out_weight, preferred_element_type=jnp.float32).astype(jnp.bfloat16),
-            "tp",
-        ).astype(jnp.float32)
+        every = lax.all_gather(attended, "sp", axis=0, tiled=True)
+        share = jnp.dot(every, w_out[layer_index], preferred_element_type=jnp.float32)
+        branch = lax.psum(share.astype(jnp.bfloat16), "tp").astype(jnp.float32)
         residual = (residual.astype(jnp.float32) + branch).astype(jnp.bfloat16)
-    return residual
+    return lax.all_to_all(residual, "sp", split_axis=0, concat_axis=1, tiled=True)
 
 
 def solution(mesh):

time: 784 us -> 527 us (0.67)
  waiting for transfers between devices: 671 us -> 350 us
  blocking collectives: 0 us -> 52.4 us
  local copies, waits for them, and re-layouts: 31.2 us -> 41.5 us
    all_gather x4 -> x2, waiting for transfers between devices: 568 us -> 54.3 us  [on_device(): every = lax.all_gather(attended, 'sp', axis=0, tiled=True)]
    reduce_scatter x0 -> x2, waiting for transfers between devices: none -> 120 us  [on_device(): lax.psum_scatter(partial.astype(jnp.bfloat16), 'sp', scatter_dimension=0,...]
    all_to_all x0 -> x1, blocking collectives: none -> 52.4 us  [on_device(): lax.all_to_all(residual, 'sp', split_axis=0, concat_axis=1, tiled=True)]
    all_to_all x0 -> x1, waiting for transfers between devices: none -> 41 us  [on_device(): lax.all_to_all(tokens, 'sp', split_axis=1, concat_axis=0, tiled=True)]
    unnamed x6 -> x10, waiting for transfers between devices: 2.64 us -> 26.1 us
    unnamed x26 -> x31, local copies, waits for them, and re-layouts: 9.34 us -> 17.4 us
    dot_general x8 -> x4, matrix products: 28.3 us -> 23.2 us  [the longest x2 15.3 us: on_device(): jnp.dot(gained, qkv_weight[layer_index], preferred_element_type=jnp.float32)]
  transfers between devices with their start and end apart: 10 -> 13, of which waited for: 6 -> 11; matrix products, arithmetic and copies ran while one was open for 7% -> 9% of each run, Pallas kernels for 0% -> 0%
where the time goes in v1:
time: 527 us
  waiting for transfers between devices  350 us (66%)
  blocking collectives  52.4 us (10%)
  local copies, waits for them, and re-layouts  41.5 us (8%)
  matrix products  36.8 us (7%)
  starting transfers between devices  16.2 us (3%)
  other arithmetic  15.8 us (3%)
  between operations  13.8 us (3%)
    reduce_scatter x2, waiting for transfers between devices, on_device(): lax.psum_scatter(partial.astype(jnp.bfloat16), 'sp', scatter_dimension=0,...  120 us
    psum x2, waiting for transfers between devices, on_device(): branch = lax.psum(share.astype(jnp.bfloat16), 'tp').astype(jnp.float32)  102 us
    all_gather x2, waiting for transfers between devices, on_device(): every = lax.all_gather(attended, 'sp', axis=0, tiled=True)  54.3 us
    all_to_all x1, blocking collectives, on_device(): lax.all_to_all(residual, 'sp', split_axis=0, concat_axis=1, tiled=True)  52.4 us
    all_to_all x1, waiting for transfers between devices, on_device(): lax.all_to_all(tokens, 'sp', split_axis=1, concat_axis=0, tiled=True)  41 us
    unnamed x10, waiting for transfers between devices  26.1 us
    unnamed x31, local copies, waits for them, and re-layouts  17.4 us
    dot_general x2, matrix products, on_device(): jnp.dot(gained, qkv_weight[layer_index], preferred_element_type=jnp.float32)  15.3 us
  transfers between devices with their start and end apart: 13, of which 11 were waited for; matrix products, arithmetic and copies ran while one was open for 9% of the time, Pallas kernels for 0%

profile of v1, /device:TPU:0, one launch (start us, length us, event | category | flops | bytes accessed | tf_op | source)
XLA Modules:
  0.0 526.5 jit_solution(16417400283458223748)
XLA Ops:
  6.5 3.1 copy.144
  9.7 6.5 %all-to-all-start = ((bf16[256,4,1024]{2,0,1:T(8,128)(2,1)}), bf16[256,4,1024]{2,0,1:T(8,128)(2,1)S(1)}, u32[]{:S(2)}, u32[]{:S(2)}) async-start(bf16[256,4,1024]{2,0,1:T(8,128)(2,1)} %bitcast.160), calls=%async_computation | async-start | bytes 4194304 | tf_op jit(solution)/shard_map/all_to_all | solution.py:65
  16.2 3.3 constant_dynamic-update-slice_fusion.2
  19.5 1.6 constant_dynamic-update-slice_fusion.1
  21.1 0.8 copy-done.6
  21.8 1.5 constant_dynamic-update-slice_fusion
  23.3 41.0 %all-to-all-done = bf16[256,4,1024]{2,0,1:T(8,128)(2,1)S(1)} async-done(((bf16[256,4,1024]{2,0,1:T(8,128)(2,1)}), bf16[256,4,1024]{2,0,1:T(8,128)(2,1)S(1)}, u32[]{:S(2)}, u32[]{:S(2)}) %all-to-all-start) | async-done | bytes 2097184 | tf_op jit(solution)/shard_map/all_to_all | solution.py:65
  64.3 2.0 multiply_reduce_fusion
  66.4 1.1 copy.76
  67.5 7.6 %convolution_convert_fusion.1 = bf16[1024,1536]{1,0:T(8,128)(2,1)} fusion(bf16[1024,1024]{1,0:T(8,128)(2,1)} %bitcast.163, bf16[2,1024,1536]{2,1,0:T(8,128)(2,1)} %constant_dynamic-update-slice_fusion), kind=kOutput, calls=%fused_computation.21 | convolution fusion | flops 3222798336 | bytes 8388608 | tf_op jit(solution)/shard_map/dot_general | solution.py:76
  75.3 0.1 subtract_add_fusion
  75.3 0.6 copy-done.8
  76.0 1.0 fusion.63
  77.0 11.6 %reduce-scatter.13.cloned.1.call-done = f32[256,1]{1,0:T(8,128)} async-done(((f32[1024,1]{1,0:T(8,128)}), f32[256,1]{1,0:T(8,128)}) %reduce-scatter.13.cloned.1.call-update) | async-done | bytes 1040
  88.6 0.9 add_rsqrt_fusion.1
  89.5 0.1 copy.79
  89.6 60.0 %reduce-scatter.9.cloned.1.call-done = bf16[256,1536]{1,0:T(8,128)(2,1)} async-done(((bf16[1024,1536]{1,0:T(8,128)(2,1)}), bf16[256,1536]{1,0:T(8,128)(2,1)}) %reduce-scatter.9.cloned.1.call-update) | async-done | bytes 786448 | tf_op jit(solution)/shard_map/reduce_scatter | solution.py:77
  149.6 1.3 multiply_convert_fusion.2
  150.9 3.6 collective-permute-start
  154.5 1.5 collective-permute-start.1
  156.0 3.9 fusion.21
  159.9 5.8 %copy.34 = f32[4,64,64,4,8]{1,2,4,3,0:T(8,128)} copy(f32[4,64,64,4,8]{2,4,3,1,0:T(8,128)} %fusion.21) | data formatting | bytes 4194304 | tf_op jit(solution)/shard_map/ijr,hrqk->hiqjk/dot_general | solution.py:92
  165.7 0.1 reshape.187
  165.8 4.0 collective-permute-done.1
  169.8 1.4 pad_maximum_fusion
  171.2 2.9 gather_fusion
  174.1 3.7 slice_bitcast_fusion.7
  177.8 1.0 fusion.79
  178.8 0.7 fusion.6
  179.5 1.0 fusion.46
  180.4 0.2 copy.37
  180.6 0.7 copy.146
  181.5 26.9 %all-gather.3.cloned.1.call-done = bf16[1024,512]{1,0:T(8,128)(2,1)} async-done(((bf16[256,512]{1,0:T(8,128)(2,1)}), bf16[1024,512]{1,0:T(8,128)(2,1)}) %all-gather.3.cloned.1.call-update) | async-done | bytes 1048592 | tf_op jit(solution)/shard_map/all_gather | solution.py:107
  208.4 4.1 convolution_convert_fusion.3
  212.6 50.8 %all-reduce.4.cloned.1.call-done = bf16[1024,1024]{1,0:T(8,128)(2,1)} async-done(((bf16[1024,1024]{1,0:T(8,128)(2,1)}), bf16[1024,1024]{1,0:T(8,128)(2,1)}) %all-reduce.4.cloned.1.call-update) | async-done | bytes 2097168 | tf_op jit(solution)/shard_map/psum | solution.py:109
  263.4 3.6 fusion.1
  267.1 1.0 copy.65
  268.2 7.6 %convolution_convert_fusion = bf16[1024,1536]{1,0:T(8,128)(2,1)} fusion(bf16[2,1024,1536]{2,1,0:T(8,128)(2,1)} %constant_dynamic-update-slice_fusion, bf16[1024,1024]{1,0:T(8,128)(2,1)} %get-tuple-element.6, f32[1024]{0:T(1024)S(1)} %bitcast.181), kind=kOutput, calls=%fused_computation.20 | convolution fusion | flops 3225944064 | bytes 8392704 | tf_op jit(solution)/shard_map/dot_general | solution.py:76
  275.9 14.3 %reduce-scatter.15.cloned.1.call-done = f32[256,1]{1,0:T(8,128)} async-done(((f32[1024,1]{1,0:T(8,128)}), f32[256,1]{1,0:T(8,128)}) %reduce-scatter.15.cloned.1.call-update) | async-done | bytes 1040
  290.2 0.9 add_rsqrt_fusion
  291.1 0.1 copy.80
  291.2 59.8 %reduce-scatter.11.cloned.1.call-done = bf16[256,1536]{1,0:T(8,128)(2,1)} async-done(((bf16[1024,1536]{1,0:T(8,128)(2,1)}), bf16[256,1536]{1,0:T(8,128)(2,1)}) %reduce-scatter.11.cloned.1.call-update) | async-done | bytes 786448 | tf_op jit(solution)/shard_map/reduce_scatter | solution.py:77
  351.1 1.3 multiply_convert_fusion.1
  352.5 2.8 collective-permute-start.2
  355.3 1.5 collective-permute-start.3
  356.8 1.0 fusion.61
  357.8 3.8 fusion.19
  361.6 5.8 %copy.41 = f32[4,64,64,4,8]{1,2,4,3,0:T(8,128)} copy(f32[4,64,64,4,8]{2,4,3,1,0:T(8,128)} %fusion.19) | data formatting | bytes 4194304 | tf_op jit(solution)/shard_map/ijr,hrqk->hiqjk/dot_general | solution.py:92
  367.4 0.1 reshape.192
  367.5 3.3 collective-permute-done.3
  370.8 0.2 pad_maximum_fusion.1
  370.9 2.8 gather_fusion.1
  373.7 3.7 slice_bitcast_fusion.5
  377.4 1.0 fusion.80
  378.4 0.7 fusion.7
  379.1 1.0 fusion.51
  380.1 0.2 copy.44
  380.3 0.7 copy.145
  381.1 27.4 %all-gather.5.cloned.1.call-done = bf16[1024,512]{1,0:T(8,128)(2,1)} async-done(((bf16[256,512]{1,0:T(8,128)(2,1)}), bf16[1024,512]{1,0:T(8,128)(2,1)}) %all-gather.5.cloned.1.call-update) | async-done | bytes 1048592 | tf_op jit(solution)/shard_map/all_gather | solution.py:107
  408.5 3.8 convolution_convert_fusion.2
  412.4 50.9 %all-reduce.6.cloned.1.call-done = bf16[1024,1024]{1,0:T(8,128)(2,1)} async-done(((bf16[1024,1024]{1,0:T(8,128)(2,1)}), bf16[1024,1024]{1,0:T(8,128)(2,1)}) %all-reduce.6.cloned.1.call-update) | async-done | bytes 2097168 | tf_op jit(solution)/shard_map/psum | solution.py:109
  463.3 2.5 fusion.2
  465.8 52.4 %all_to_all.32 = bf16[4,256,1024]{2,1,0:T(8,128)(2,1)S(1)} all-to-all(bf16[4,256,1024]{2,1,0:T(8,128)(2,1)S(1)} %bitcast.159), channel_id=1, replica_groups=mesh['grp'=2,'sp'=4,'tp'=4] {'sp'}, dimensions={0} | all-to-all | bytes 4194304 | tf_op jit(solution)/shard_map/all_to_all | solution.py:111
  518.2 1.5 copy.74
  (50 shorter events, 0.7 us)
Async XLA Ops:
  9.7 6.5 %copy-start.7 = (bf16[2,4096]{1,0:T(2,128)(2,1)S(1)}, bf16[2,4096]{1,0:T(2,128)(2,1)}, u32[]{:S(2)}) copy-start(bf16[2,4096]{1,0:T(2,128)(2,1)} %param.8) | copy-start | bytes 49156
  9.7 54.7 %all-to-all-start = ((bf16[256,4,1024]{2,0,1:T(8,128)(2,1)}), bf16[256,4,1024]{2,0,1:T(8,128)(2,1)S(1)}, u32[]{:S(2)}, u32[]{:S(2)}) async-start(bf16[256,4,1024]{2,0,1:T(8,128)(2,1)} %bitcast.160), calls=%async_computation | async-start | bytes 4194304 | tf_op jit(solution)/shard_map/all_to_all | solution.py:65
  16.1 72.4 %reduce-scatter.13.cloned.1.call-start = ((), (), s32[]{:S(2)}) async-start(), calls=%async_computation.12 | async-start | bytes 655360
  16.2 3.3 copy-start.5
  19.5 2.3 copy-start.6
  64.3 2.0 copy-start
  67.4 82.1 %reduce-scatter.9.cloned.1.call-start = ((), (), s32[]{:S(2)}) async-start(), calls=%async_computation.6 | async-start | bytes 3932160 | tf_op jit(solution)/shard_map/reduce_scatter | solution.py:77
  75.1 0.8 copy-start.8
  75.2 133.2 %all-gather.3.cloned.1.call-start = ((), (), s32[]{:S(2)}) async-start(), calls=%async_computation.7 | async-start | bytes 1310720 | tf_op jit(solution)/shard_map/all_gather | solution.py:107
  150.9 14.9 %collective-permute-start = (bf16[4,64,1024]{2,1,0:T(8,128)(2,1)S(1)}, bf16[4,64,1024]{2,1,0:T(8,128)(2,1)}, u32[]{:S(2)}, u32[]{:S(2)}) collective-permute-start(bf16[4,64,1024]{2,1,0:T(8,128)(2,1)S(1)} %bitcast.165), channel_id=1, source_target_pairs={{0,4},{4,8},{8,12},{1,5},{5,9},{9,13},{2,6},{6,10},{10,14},{3,7},{... | collective-permute-start | bytes 1572872 | tf_op jit(solution)/shard_map/ppermute | solution.py:21
  154.5 15.3 %collective-permute-start.1 = (bf16[4,64,1024]{2,1,0:T(8,128)(2,1)S(1)}, bf16[4,64,1024]{2,1,0:T(8,128)(2,1)}, u32[]{:S(2)}, u32[]{:S(2)}) collective-permute-start(bf16[4,64,1024]{2,1,0:T(8,128)(2,1)S(1)} %bitcast.166), channel_id=1, source_target_pairs={{4,0},{8,4},{12,8},{5,1},{9,5},{13,9},{6,2},{10,6},{14,10},{7,3},{... | collective-permute-start | bytes 1572872 | tf_op jit(solution)/shard_map/ppermute | solution.py:24
  174.1 3.7 copy-start.2
  181.4 82.0 %all-reduce.4.cloned.1.call-start = ((), (), s32[]{:S(2)}) async-start(), calls=%async_computation.8 | async-start | bytes 4194304 | tf_op jit(solution)/shard_map/psum | solution.py:109
  212.5 50.9 %copy-start.1 = (bf16[256,4,1024]{2,0,1:T(8,128)(2,1)S(1)}, bf16[256,4,1024]{2,0,1:T(8,128)(2,1)}, u32[]{:S(2)}) copy-start(bf16[256,4,1024]{2,0,1:T(8,128)(2,1)} %copy-done) | copy-start | bytes 6291460
  212.5 77.7 %reduce-scatter.15.cloned.1.call-start = ((), (), s32[]{:S(2)}) async-start(), calls=%async_computation.13 | async-start | bytes 655360
  268.1 82.9 %reduce-scatter.11.cloned.1.call-start = ((), (), s32[]{:S(2)}) async-start(), calls=%async_computation.9 | async-start | bytes 3932160 | tf_op jit(solution)/shard_map/reduce_scatter | solution.py:77
  275.8 132.7 %all-gather.5.cloned.1.call-start = ((), (), s32[]{:S(2)}) async-start(), calls=%async_computation.10 | async-start | bytes 1310720 | tf_op jit(solution)/shard_map/all_gather | solution.py:107
  352.5 15.0 %collective-permute-start.2 = (bf16[4,64,1024]{2,1,0:T(8,128)(2,1)S(1)}, bf16[4,64,1024]{2,1,0:T(8,128)(2,1)S(1)}, u32[]{:S(2)}, u32[]{:S(2)}) collective-permute-start(bf16[4,64,1024]{2,1,0:T(8,128)(2,1)S(1)} %bitcast.168), channel_id=1, source_target_pairs={{0,4},{4,8},{8,12},{1,5},{5,9},{9,13},{2,6},{6,10},{10,14},{3,7},{... | collective-permute-start | bytes 1572872 | tf_op jit(solution)/shard_map/ppermute | solution.py:21
  355.3 15.5 %collective-permute-start.3 = (bf16[4,64,1024]{2,1,0:T(8,128)(2,1)S(1)}, bf16[4,64,1024]{2,1,0:T(8,128)(2,1)S(1)}, u32[]{:S(2)}, u32[]{:S(2)}) collective-permute-start(bf16[4,64,1024]{2,1,0:T(8,128)(2,1)S(1)} %bitcast.169), channel_id=1, source_target_pairs={{4,0},{8,4},{12,8},{5,1},{9,5},{13,9},{6,2},{10,6},{14,10},{7,3},{... | collective-permute-start | bytes 1572872 | tf_op jit(solution)/shard_map/ppermute | solution.py:24
  373.7 3.7 copy-start.3
  379.1 29.4 %copy-start.9 = (bf16[2,512,1024]{2,1,0:T(8,128)(2,1)S(1)}, bf16[2,512,1024]{2,1,0:T(8,128)(2,1)}, u32[]{:S(2)}) copy-start(bf16[2,512,1024]{2,1,0:T(8,128)(2,1)} %param.12) | copy-start | bytes 6291460
  381.1 82.2 %all-reduce.6.cloned.1.call-start = ((), (), s32[]{:S(2)}) async-start(), calls=%async_computation.11 | async-start | bytes 4194304 | tf_op jit(solution)/shard_map/psum | solution.py:109
  412.3 50.9 %copy-start.4 = (bf16[1024,1024]{1,0:T(8,128)(2,1)S(1)}, bf16[1024,1024]{1,0:T(8,128)(2,1)}, u32[]{:S(2)}) copy-start(bf16[1024,1024]{1,0:T(8,128)(2,1)} %get-tuple-element.6) | copy-start | bytes 6291460
Sparse Core Ops, SparseCore 0:
  67.6 20.9 reduce-scatter.12
  90.9 58.6 reduce-scatter.8
  181.5 26.7 all-gather.2
  212.6 50.7 all-reduce.3
  268.2 21.9 reduce-scatter.14
  292.4 58.6 reduce-scatter.10
  381.2 27.2 all-gather.4
  412.5 50.7 all-reduce.5

commit v2 on v1

--- a/solution.py
+++ b/solution.py
@@ -1,6 +1,10 @@
+import functools
+
 import jax
 import jax.numpy as jnp
 from jax import lax
+from jax.experimental import pallas as pl
+from jax.experimental.pallas import tpu as pltpu
 from jax.sharding import PartitionSpec as P
 
 HD = 128
@@ -32,7 +36,7 @@
     return (scaled * gain.astype(jnp.float32)).astype(jnp.bfloat16)
 
 
-def on_device(tokens, norm_gain, w_query, w_key, w_value, w_out, offset_bias):
+def general(tokens, norm_gain, w_query, w_key, w_value, w_out, offset_bias):
     sp_count = lax.axis_size("sp")
     sp_index = lax.axis_index("sp")
     tok_rows = tokens.shape[0]
@@ -111,6 +115,472 @@
     return lax.all_to_all(residual, "sp", split_axis=0, concat_axis=1, tiled=True)
 
 
+MESH = pl.DeviceIdType.MESH
+VMEM_MOST = 60 * 2**20
+CHUNK = 128
+PIECE = 64
+LAG = 2
+
+
+def greet(peers):
+    barrier = pltpu.get_barrier_semaphore()
+    for axis, index in peers:
+        pl.semaphore_signal(barrier, inc=1, device_id={axis: index}, device_id_type=MESH)
+    pl.semaphore_wait(barrier, len(peers))
+
+
+def remote(src, dst, send, recv, axis, index):
+    return pltpu.make_async_remote_copy(
+        src_ref=src, dst_ref=dst, send_sem=send, recv_sem=recv,
+        device_id={axis: index}, device_id_type=MESH,
+    )
+
+
+def span(start, size):
+    return pl.ds(pl.multiple_of(start, size), size)
+
+
+def spread_kernel(n, tok_ref, x_ref, send, recv, far_send, far_recv):
+    me, t = lax.axis_index("sp"), lax.axis_index("tp")
+    half = lax.rem(t, 2)
+    partner = t + 1 - 2 * half
+    rows, width = tok_ref.shape[0], tok_ref.shape[1] // n
+    part = width // 2
+    greet([("sp", lax.rem(me + k, n)) for k in range(1, n)] + [("tp", partner)])
+    lanes = span(half * part, part)
+    sent = []
+    for k in range(1, n):
+        to = lax.rem(me + k, n)
+        copy = remote(
+            tok_ref.at[:, span(to * width + half * part, part)],
+            x_ref.at[span(me * rows, rows), lanes],
+            send.at[k - 1], recv.at[k - 1], "sp", to,
+        )
+        copy.start()
+        sent.append(copy)
+    x_ref[span(me * rows, rows), :] = tok_ref[:, span(me * width, width)]
+    passed = []
+    for k in range(1, n):
+        source = lax.rem(me + n - k, n)
+        sent[k - 1].wait_recv()
+        here = x_ref.at[span(source * rows, rows), lanes]
+        copy = remote(here, here, far_send.at[k - 1], far_recv.at[k - 1], "tp", partner)
+        copy.start()
+        passed.append(copy)
+    for k in range(n - 1):
+        sent[k].wait_send()
+        passed[k].wait()
+
+
+def project_kernel(
+    n, layer, features, x_ref, gain_ref, wq_ref, wk_ref, wv_ref, out_ref,
+    gained, inbox, outbox, acc, sq_own, sq_in, inverse,
+    send, recv, sq_send, sq_recv,
+):
+    me = lax.axis_index("sp")
+    tokens, width = x_ref.shape
+    cols = wq_ref.shape[1] // 2
+    pieces = tokens // PIECE
+    greet([("sp", lax.rem(me + k, n)) for k in range(1, n)])
+    gain = gain_ref[pl.ds(layer, 1), span(me * width, width)].astype(jnp.float32)
+    ones = jnp.ones((8, width), jnp.float32)
+
+    @pl.loop(0, tokens // CHUNK)
+    def _(i):
+        rows = span(i * CHUNK, CHUNK)
+        wide = x_ref[rows, :].astype(jnp.float32)
+        gained[rows, :] = (wide * gain).astype(jnp.bfloat16)
+        sq_own[:, rows] = lax.dot_general(
+            ones, wide * wide, (((1,), (1,)), ((), ())),
+            precision=lax.Precision.HIGHEST, preferred_element_type=jnp.float32,
+        )
+
+    ends = (n - 1, 0)
+    for e, end in enumerate(ends):
+        @pl.when(me != end)
+        def _(e=e, end=end):
+            remote(sq_own, sq_in.at[me], sq_send.at[e], sq_recv.at[me], "sp", end).start()
+
+    at_end = (me == 0) | (me == n - 1)
+
+    @pl.when(at_end)
+    def _():
+        for k in range(1, n):
+            source = lax.rem(me + k, n)
+            remote(sq_own, sq_in.at[source], sq_send.at[0], sq_recv.at[source], "sp", source).wait_recv()
+        sq_in[me] = sq_own[...]
+
+        @pl.loop(0, tokens // CHUNK)
+        def _(i):
+            rows = span(i * CHUNK, CHUNK)
+            total = sq_in[0, :, rows]
+            for k in range(1, n):
+                total = total + sq_in[k, :, rows]
+            scaled = lax.rsqrt(total / features + norm_eps)
+            inverse[rows, :] = jnp.concatenate([scaled] * (CHUNK // 8), axis=0).T
+
+    def flow(way, piece):
+        place = me if way == 0 else n - 1 - me
+        after = me + 1 if way == 0 else me - 1
+        rows = span(piece * PIECE, PIECE)
+        lo = (1 - way) * cols
+        for j, w_ref in enumerate((wq_ref, wk_ref, wv_ref)):
+            acc[:, j * cols:(j + 1) * cols] = jnp.dot(
+                gained[rows, :], w_ref[:, lo:lo + cols], preferred_element_type=jnp.float32
+            )
+
+        def copy():
+            return remote(
+                outbox.at[way, rows, :], inbox.at[way, rows, :],
+                send.at[way, piece], recv.at[way, piece], "sp", after,
+            )
+
+        @pl.when(place > 0)
+        def _():
+            copy().wait_recv()
+            acc[...] += inbox[way, rows, :].astype(jnp.float32)
+
+        @pl.when(place < n - 1)
+        def _():
+            outbox[way, rows, :] = acc[...].astype(jnp.bfloat16)
+            copy().start()
+
+        @pl.when(place == n - 1)
+        def _():
+            out_ref[rows, :] = (acc[...] * inverse[rows, :1]).astype(jnp.bfloat16)
+
+    @pl.loop(0, pieces + (n - 1) * LAG)
+    def _(step):
+        for way in range(2):
+            place = me if way == 0 else n - 1 - me
+            piece = step - place * LAG
+
+            @pl.when((piece >= 0) & (piece < pieces))
+            def _(way=way, piece=piece):
+                flow(way, piece)
+
+    @pl.when(jnp.logical_not(at_end))
+    def _():
+        out_ref[...] = jnp.zeros_like(out_ref)
+
+    for e, end in enumerate(ends):
+        @pl.when(me != end)
+        def _(e=e, end=end):
+            remote(sq_own, sq_in.at[me], sq_send.at[e], sq_recv.at[me], "sp", end).wait_send()
+
+            @pl.loop(0, pieces)
+            def _(i):
+                rows = span(i * PIECE, PIECE)
+                remote(
+                    outbox.at[e, rows, :], inbox.at[e, rows, :],
+                    send.at[e, i], recv.at[e, i], "sp", end,
+                ).wait_send()
+
+
+def attend_kernel(heads, rows, scale, mine_ref, bias_ref, out_ref):
+    cols = heads * HD
+    for h in range(heads):
+        for r in range(rows):
+            first = min(max(r - KR // 2, 0), rows - KR)
+            q = mine_ref[r * GRID_W:(r + 1) * GRID_W, h * HD:(h + 1) * HD]
+            band = slice(first * GRID_W, (first + KR) * GRID_W)
+            k = mine_ref[band, cols + h * HD:cols + (h + 1) * HD]
+            v = mine_ref[band, 2 * cols + h * HD:2 * cols + (h + 1) * HD]
+            scores = lax.dot_general(
+                q, k, (((1,), (1,)), ((), ())), preferred_element_type=jnp.float32
+            )
+            scores = scores * scale + bias_ref[h, first - r + KR - 1]
+            scores = jnp.exp(scores - jnp.max(scores, axis=-1, keepdims=True))
+            weights = scores / jnp.sum(scores, axis=-1, keepdims=True)
+            out = jnp.dot(weights.astype(jnp.bfloat16), v, preferred_element_type=jnp.float32)
+            out_ref[r * GRID_W:(r + 1) * GRID_W, h * HD:(h + 1) * HD] = out.astype(jnp.bfloat16)
+
+
+def combine_kernel(
+    n, m, last, att_ref, x_ref, w_ref, out_ref,
+    box, give, take, pair, cross_in, fresh,
+    send, recv, give_s, give_r, cross_s, cross_r, fresh_s, fresh_r, far_s, far_r,
+):
+    me, t = lax.axis_index("sp"), lax.axis_index("tp")
+    half = lax.rem(t, 2)
+    partner = t + 1 - 2 * half
+    cross = lax.rem(t + m // 2, m)
+    tokens, width = x_ref.shape
+    cols = att_ref.shape[1]
+    part = width // 2
+    chunks = tokens // CHUNK
+    per = chunks // n
+    lanes = span(half * part, part)
+    other = span((1 - half) * part, part)
+    greet(
+        [("sp", lax.rem(me + k, n)) for k in range(1, n)] + [("tp", partner), ("tp", cross)]
+    )
+
+    def where(step):
+        return span((lax.rem(step, n) * per + step // n) * CHUNK, CHUNK)
+
+    def hop(way, step, source=None):
+        rows = where(step)
+        src = box.at[way, rows, :] if source is None else source.at[rows, :]
+        after = me + 1 if way == 0 else me - 1
+        return remote(src, box.at[way, rows, :], send.at[way, step], recv.at[way, step], "sp", after)
+
+    for way, start in ((0, 0), (1, n - 1)):
+        @pl.when(me == start)
+        def _(way=way):
+            @pl.loop(0, chunks)
+            def _(i):
+                hop(way, i, att_ref).start()
+            box[way] = att_ref[...]
+
+    def onward(way, step):
+        place = me if way == 0 else n - 1 - me
+
+        @pl.when(place > 0)
+        def _():
+            hop(way, step).wait_recv()
+
+            @pl.when(place < n - 1)
+            def _():
+                hop(way, step).start()
+
+    def forward(step):
+        @pl.when(me < n // 2)
+        def _():
+            onward(0, step)
+            onward(1, step)
+
+        @pl.when(me >= n // 2)
+        def _():
+            onward(1, step)
+            onward(0, step)
+
+    def give_copy(step):
+        rows = where(step)
+        return remote(give.at[rows, :], take.at[rows, :], give_s.at[step], give_r.at[step], "tp", partner)
+
+    def cross_copy(step):
+        rows = where(step)
+        return remote(
+            pair.at[rows, :], cross_in.at[rows, :], cross_s.at[step], cross_r.at[step], "tp", cross
+        )
+
+    def multiply(step):
+        rows = where(step)
+
+        def share(at):
+            return jnp.dot(
+                box[0, rows, :], w_ref[:cols, at], preferred_element_type=jnp.float32
+            ) + jnp.dot(box[1, rows, :], w_ref[cols:, at], preferred_element_type=jnp.float32)
+
+        give[rows, :] = share(other).astype(jnp.bfloat16)
+        give_copy(step).start()
+        pair[rows, :] = share(lanes).astype(jnp.bfloat16)
+
+    def meet(step):
+        rows = where(step)
+        give_copy(step).wait_recv()
+        pair[rows, :] = (
+            pair[rows, :].astype(jnp.float32) + take[rows, :].astype(jnp.float32)
+        ).astype(jnp.bfloat16)
+        cross_copy(step).start()
+
+    def fresh_copy(step):
+        rows = where(step)
+        if not last:
+            return remote(
+                fresh.at[rows, :], out_ref.at[rows, lanes], fresh_s.at[step], fresh_r.at[step], "tp", partner
+            )
+        return remote(
+            fresh.at[rows, :],
+            out_ref.at[span(step // n * CHUNK, CHUNK), span(me * width + half * part, part)],
+            fresh_s.at[step], fresh_r.at[me, step // n], "sp", lax.rem(step, n),
+        )
+
+    def finish(step):
+        rows = where(step)
+        cross_copy(step).wait_recv()
+        branch = pair[rows, :].astype(jnp.float32) + cross_in[rows, :].astype(jnp.float32)
+        new = (x_ref[rows, lanes].astype(jnp.float32) + branch).astype(jnp.bfloat16)
+        if not last:
+            fresh[rows, :] = new
+            fresh_copy(step).start()
+            out_ref[rows, lanes] = new
+            return
+
+        @pl.when(lax.rem(step, n) == me)
+        def _():
+            out_ref[span(step // n * CHUNK, CHUNK), span(me * width + half * part, part)] = new
+
+        @pl.when(lax.rem(step, n) != me)
+        def _():
+            fresh[rows, :] = new
+            fresh_copy(step).start()
+
+    stages = ((forward, 0), (multiply, 1), (meet, 2), (finish, 4))
+
+    @pl.loop(0, chunks + 4)
+    def _(step):
+        for stage, late in stages:
+            at = step - late
+
+            @pl.when((at >= 0) & (at < chunks))
+            def _(stage=stage, at=at):
+                stage(at)
+
+    if last:
+        def far_copy(source, q):
+            here = out_ref.at[span(q * CHUNK, CHUNK), span(source * width + half * part, part)]
+            return remote(here, here, far_s.at[source, q], far_r.at[source, q], "tp", partner)
+
+        for q in range(per):
+            for k in range(n):
+                source = lax.rem(me + k, n)
+                if k > 0:
+                    here = out_ref.at[span(q * CHUNK, CHUNK), span(source * width + half * part, part)]
+                    remote(
+                        here, here, far_s.at[source, q], fresh_r.at[source, q], "sp", source
+                    ).wait_recv()
+                far_copy(source, q).start()
+        for q in range(per):
+            for k in range(n):
+                source = lax.rem(me + k, n)
+                there = out_ref.at[span(q * CHUNK, CHUNK), span(source * width + (1 - half) * part, part)]
+                remote(there, there, far_s.at[source, q], far_r.at[source, q], "tp", partner).wait_recv()
+                far_copy(source, q).wait_send()
+
+    @pl.loop(0, chunks)
+    def _(i):
+        give_copy(i).wait_send()
+        cross_copy(i).wait_send()
+        if not last:
+            rows = where(i)
+            fresh_copy(i).wait_send()
+            remote(
+                fresh.at[rows, :], out_ref.at[rows, other], fresh_s.at[i], fresh_r.at[i], "tp", partner
+            ).wait_recv()
+        else:
+            @pl.when(lax.rem(i, n) != me)
+            def _():
+                fresh_copy(i).wait_send()
+        for way, end in ((0, n - 1), (1, 0)):
+            @pl.when(me != end)
+            def _(way=way):
+                hop(way, i).wait_send()
+
+
+def vmem():
+    return pl.BlockSpec(memory_space=pltpu.VMEM)
+
+
+def of_layer(array, layer):
+    rest = array.shape[1:]
+    return pl.BlockSpec((None, *rest), lambda i: (layer, *(0 for _ in rest)))
+
+
+def params(identity):
+    return pltpu.CompilerParams(
+        collective_id=identity, has_side_effects=True, vmem_limit_bytes=VMEM_MOST
+    )
+
+
+def staged(tokens, norm_gain, w_query, w_key, w_value, w_out, offset_bias):
+    n, m = lax.axis_size("sp"), lax.axis_size("tp")
+    me = lax.axis_index("sp")
+    own, features = tokens.shape
+    width, total = features // n, own * n
+    grid_rows = total // GRID_W
+    heads = offset_bias.shape[1] // 2
+    cols = heads * HD
+    dma = pltpu.SemaphoreType.DMA
+    bf16, f32 = jnp.bfloat16, jnp.float32
+
+    columns = jnp.arange(GRID_W, dtype=jnp.int32)
+    col_first = jnp.clip(columns - KC // 2, 0, GRID_W - KC)
+    inside = (columns[None, :] >= col_first[:, None]) & (columns[None, :] < col_first[:, None] + KC)
+    offset = jnp.clip(columns[None, :] - columns[:, None], 1 - KC, KC - 1) + KC - 1
+    onehot = (
+        jnp.arange(2 * KC - 1, dtype=jnp.int32)[:, None, None] == offset[None, :, :]
+    ).astype(f32)
+    table = lax.dynamic_slice_in_dim(offset_bias, jnp.where(me == n - 1, heads, 0), heads, 1)
+    table = jnp.stack([table[:, :, a:a + KR] for a in range(KR)], axis=2)
+    bias = jnp.einsum("lhajo,oqk->lhaqjk", table, onehot, precision=lax.Precision.HIGHEST)
+    bias = jnp.where(inside[:, None, :], bias, -jnp.inf)
+    bias = bias.reshape(LAYERS, heads, KR, GRID_W, KR * GRID_W)
+
+    x = pl.pallas_call(
+        functools.partial(spread_kernel, n),
+        out_shape=jax.ShapeDtypeStruct((total, width), bf16),
+        in_specs=[vmem()],
+        grid=(1,),
+        out_specs=vmem(),
+        scratch_shapes=[dma((n - 1,))] * 4,
+        compiler_params=params(1),
+        name="spread",
+    )(tokens)
+    pieces, chunks = total // PIECE, total // CHUNK
+    for layer in range(LAYERS):
+        last = layer == LAYERS - 1
+        mine = pl.pallas_call(
+            functools.partial(project_kernel, n, layer, features),
+            out_shape=jax.ShapeDtypeStruct((total, 3 * cols), bf16),
+            in_specs=[vmem(), vmem()] + [of_layer(w, layer) for w in (w_query, w_key, w_value)],
+            grid=(1,),
+            out_specs=vmem(),
+            scratch_shapes=[
+                pltpu.VMEM((total, width), bf16),
+                pltpu.VMEM((2, total, 3 * cols), bf16),
+                pltpu.VMEM((2, total, 3 * cols), bf16),
+                pltpu.VMEM((PIECE, 3 * cols), f32),
+                pltpu.VMEM((8, total), f32),
+                pltpu.VMEM((n, 8, total), f32),
+                pltpu.VMEM((total, CHUNK), f32),
+                dma((2, pieces)), dma((2, pieces)), dma((2,)), dma((n,)),
+            ],
+            compiler_params=params(2 + 2 * layer),
+            name="project",
+        )(x, norm_gain, w_query, w_key, w_value)
+        attended = pl.pallas_call(
+            functools.partial(attend_kernel, heads, grid_rows, HD ** (-0.5)),
+            out_shape=jax.ShapeDtypeStruct((total, cols), bf16),
+            in_specs=[vmem(), of_layer(bias, layer)],
+            grid=(1,),
+            out_specs=vmem(),
+            compiler_params=pltpu.CompilerParams(vmem_limit_bytes=VMEM_MOST),
+            name="attend",
+        )(mine, bias)
+        x = pl.pallas_call(
+            functools.partial(combine_kernel, n, m, last),
+            out_shape=jax.ShapeDtypeStruct((own, features) if last else (total, width), bf16),
+            in_specs=[vmem(), vmem(), of_layer(w_out, layer)],
+            grid=(1,),
+            out_specs=vmem(),
+            scratch_shapes=[
+                pltpu.VMEM((2, total, cols), bf16),
+                *[pltpu.VMEM((total, width // 2), bf16)] * 5,
+                dma((2, chunks)), dma((2, chunks)),
+                *[dma((chunks,))] * 4,
+                dma((chunks,)),
+                dma((n, chunks // n)) if last else dma((chunks,)),
+                dma((n, chunks // n)), dma((n, chunks // n)),
+            ],
+            compiler_params=params(3 + 2 * layer),
+            name="combine",
+        )(attended, x, w_out)
+    return x
+
+
+def on_device(tokens, norm_gain, w_query, w_key, w_value, w_out, offset_bias):
+    n, m = lax.axis_size("sp"), lax.axis_size("tp")
+    own, features = tokens.shape
+    total, width = own * n, features // n
+    fits = total * (6 * width + 8 * w_query.shape[2]) * 2 < VMEM_MOST // 2
+    even = offset_bias.shape[1] % 2 == 0 and m == 4 and n > 1
+    if fits and even and own % CHUNK == 0 and width % 256 == 0:
+        return staged(tokens, norm_gain, w_query, w_key, w_value, w_out, offset_bias)
+    return general(tokens, norm_gain, w_query, w_key, w_value, w_out, offset_bias)
+
+
 def solution(mesh):
     return jax.shard_map(
         on_device,

time: 527 us -> 334 us (0.63)
  waiting for transfers between devices: 350 us -> 0 us
  Pallas kernels: 0 us -> 306 us
  blocking collectives: 52.4 us -> 0 us
  matrix products: 36.8 us -> 5.63 us
  local copies, waits for them, and re-layouts: 41.5 us -> 18.3 us
  starting transfers between devices: 16.2 us -> 0 us
  other arithmetic: 15.8 us -> 0.1 us
  between operations: 13.8 us -> 0.13 us
    pallas_call x0 -> x7, Pallas kernels: none -> 306 us  [the longest x2 126 us: staged(): pl.pallas_call(functools.partial(project_kernel, n, layer, features), out...]
    reduce_scatter x2 -> x0, waiting for transfers between devices: 120 us -> none  [on_device(): lax.psum_scatter(partial.astype(jnp.bfloat16), 'sp', scatter_dimension=0,...]
    psum x2 -> x0, waiting for transfers between devices: 102 us -> none  [on_device(): branch = lax.psum(share.astype(jnp.bfloat16), 'tp').astype(jnp.float32)]
    all_gather x2 -> x0, waiting for transfers between devices: 54.3 us -> none  [on_device(): every = lax.all_gather(attended, 'sp', axis=0, tiled=True)]
    all_to_all x1 -> x0, blocking collectives: 52.4 us -> none  [on_device(): lax.all_to_all(residual, 'sp', split_axis=0, concat_axis=1, tiled=True)]
    all_to_all x1 -> x0, waiting for transfers between devices: 41 us -> none  [on_device(): lax.all_to_all(tokens, 'sp', split_axis=1, concat_axis=0, tiled=True)]
    dot_general x12 -> x1, matrix products: 36.8 us -> 5.63 us  [staged(): jnp.einsum('lhajo,oqk->lhaqjk', table, onehot, precision=lax.Precision.HI...]
    unnamed x10 -> x0, waiting for transfers between devices: 26.1 us -> none
  transfers between devices with their start and end apart: 13 -> 0, of which waited for: 11 -> 0; matrix products, arithmetic and copies ran while one was open for 9% -> 0% of each run, Pallas kernels for 0% -> 0%
where the time goes in v2:
time: 334 us; the launch traced here: 330 us
  Pallas kernels  306 us (92%)
  local copies, waits for them, and re-layouts  18.3 us (5%)
  matrix products  5.63 us (2%)
    pallas_call x2, Pallas kernels, staged(): pl.pallas_call(functools.partial(project_kernel, n, layer, features), out...  126 us
    pallas_call x2, Pallas kernels, staged(): pl.pallas_call(functools.partial(combine_kernel, n, m, last), out_shape=j...  125 us
    pallas_call x1, Pallas kernels, staged(): pl.pallas_call(functools.partial(spread_kernel, n), out_shape=jax.ShapeDt...  28 us
    pallas_call x2, Pallas kernels, staged(): pl.pallas_call(functools.partial(attend_kernel, heads, grid_rows, HD ** (...  27.5 us
    reshape x2, local copies, waits for them, and re-layouts, staged(): bias = bias.reshape(LAYERS, heads, KR, GRID_W, KR * GRID_W)  14 us

profile of v2, /device:TPU:0, one launch (start us, length us, event | category | flops | bytes accessed | tf_op | source)
XLA Modules:
  0.0 330.1 jit_solution(10404792191586805175)
XLA Ops:
  0.0 1.1 constant_dynamic-slice_fusion.7
  1.2 0.1 fusion.4
  1.4 5.6 %select_bitcast_fusion = f32[2,2,8,64,8,64]{5,4,2,1,0,3:T(8,128)} fusion(pred[64,64]{1,0:T(8,128)(4,1)S(1)} %fusion.4, s32[64,64]{1,0:T(8,128)S(1)} %clamp_add_fusion, f32[2,2,8,8,31]{4,3,2,1,0:T(8,128)S(1)} %constant_dynamic-update-slice_fusion), kind=kOutput, calls=%fused_computation | convolution fusion | flops 391245824 | bytes 4246528 | tf_op jit(solution)/shard_map/lhajo,oqk->lhaqjk/dot_general | solution.py:507
  7.0 7.5 %reshape.29 = f32[2,2,8,64,512]{4,2,1,0,3:T(8,128)} reshape(f32[2,2,8,64,8,64]{5,4,2,1,0,3:T(8,128)} %select_bitcast_fusion) | data formatting | bytes 8388608 | tf_op jit(solution)/shard_map/reshape | solution.py:509
  14.5 6.5 %copy.18.bias_ref = f32[2,2,8,64,512]{4,3,2,1,0:T(8,128)} copy(f32[2,2,8,64,512]{4,2,1,0,3:T(8,128)} %reshape.29) | data formatting | bytes 8388608 | tf_op jit(solution)/shard_map/reshape | solution.py:509
  21.0 28.0 %spread.1.x_ref = bf16[1024,1024]{1,0:T(8,128)(2,1)} custom-call(bf16[256,4096]{1,0:T(8,128)(2,1)} %tok_ref.1), custom_call_target="tpu_custom_call" | custom-call | tf_op jit(solution)/shard_map/spread/pallas_call | solution.py:511
  49.0 65.8 %project.2.mine_ref = bf16[1024,768]{1,0:T(8,128)(2,1)} custom-call(bf16[1024,1024]{1,0:T(8,128)(2,1)} %spread.1.x_ref, bf16[2,4096]{1,0:T(2,128)(2,1)} %gain_ref.3, bf16[2,1024,512]{2,1,0:T(8,128)(2,1)} %wq_ref.3, bf16[2,1024,512]{2,1,0:T(8,128)(2,1)} %wk_ref.3, bf16[2,1024,512]{2,1,0:T(8,128)(2,1)} %wv_ref.3), custom_call_target="tpu_custom_call" | custom-call | tf_op jit(solution)/shard_map/project/pallas_call | solution.py:524
  114.9 13.7 %attend.2.att_ref = bf16[1024,256]{1,0:T(8,128)(2,1)} custom-call(bf16[1024,768]{1,0:T(8,128)(2,1)} %project.2.mine_ref, f32[2,2,8,64,512]{4,3,2,1,0:T(8,128)} %copy.18.bias_ref), custom_call_target="tpu_custom_call" | custom-call | tf_op jit(solution)/shard_map/attend/pallas_call | solution.py:543
  128.6 55.8 %combine.2.x_ref = bf16[1024,1024]{1,0:T(8,128)(2,1)} custom-call(bf16[1024,256]{1,0:T(8,128)(2,1)} %attend.2.att_ref, bf16[1024,1024]{1,0:T(8,128)(2,1)} %spread.1.x_ref, bf16[2,512,1024]{2,1,0:T(8,128)(2,1)} %w_ref.3), custom_call_target="tpu_custom_call" | custom-call | tf_op jit(solution)/shard_map/combine/pallas_call | solution.py:552
  184.4 59.9 %project.3.mine_ref = bf16[1024,768]{1,0:T(8,128)(2,1)} custom-call(bf16[1024,1024]{1,0:T(8,128)(2,1)} %combine.2.x_ref, bf16[2,4096]{1,0:T(2,128)(2,1)} %gain_ref.3, bf16[2,1024,512]{2,1,0:T(8,128)(2,1)} %wq_ref.3, bf16[2,1024,512]{2,1,0:T(8,128)(2,1)} %wk_ref.3, bf16[2,1024,512]{2,1,0:T(8,128)(2,1)} %wv_ref.3), custom_call_target="tpu_custom_call" | custom-call | tf_op jit(solution)/shard_map/project/pallas_call | solution.py:524
  244.4 13.7 %attend.3.att_ref = bf16[1024,256]{1,0:T(8,128)(2,1)} custom-call(bf16[1024,768]{1,0:T(8,128)(2,1)} %project.3.mine_ref, f32[2,2,8,64,512]{4,3,2,1,0:T(8,128)} %copy.18.bias_ref), custom_call_target="tpu_custom_call" | custom-call | tf_op jit(solution)/shard_map/attend/pallas_call | solution.py:543
  258.1 68.8 %combine.3 = bf16[256,4096]{1,0:T(8,128)(2,1)} custom-call(bf16[1024,256]{1,0:T(8,128)(2,1)} %attend.3.att_ref, bf16[1024,1024]{1,0:T(8,128)(2,1)} %combine.2.x_ref, bf16[2,512,1024]{2,1,0:T(8,128)(2,1)} %w_ref.3), custom_call_target="tpu_custom_call" | custom-call | tf_op jit(solution)/shard_map/combine/pallas_call | solution.py:552
  327.0 3.1 copy.60
  (10 shorter events, 0.0 us)
